TPU v7x, 256 devices: a whole 4x4x8 slice. The times are simulated.
256 devices in a mesh: ep: 16 (over y, x), tp: 16 (over z, core).
Axes of the slice: x: 4, y: 4, z: 8, core: 2. Of those that a mesh axis runs over, the one named last changes fastest.
Arguments:
- queries: bfloat16 [16384, 1024], P('ep', 'tp'), may hold values from -8 to 8
- keys: bfloat16 [16384, 256], P('ep'), may hold values from -8 to 8
- values: bfloat16 [16384, 256], P('ep'), may hold values from -6 to 6
- query_gain: float32 [64], replicated, may hold values from 1 to 10
- key_gain: float32 [64], replicated, may hold values from 1 to 10
- moe_input: bfloat16 [12288, 2048], P(('ep', 'tp')), may hold values from -6 to 6
- expert_ids: int32 [12288, 2], P('ep'), may hold values from 0 to 15, all different within a row; in each aligned block of 48 rows (0 to 47, 48 to 95, ...) at most 7 rows name the same one
- route_weight: float32 [12288, 2], P('ep'), may hold values from 0.2 to 1
- gate_weight: bfloat16 [16, 2048, 7168], P('ep', None, 'tp'), may hold values from -0.125 to 0.125
- up_weight: bfloat16 [16, 2048, 7168], P('ep', None, 'tp'), may hold values from -0.125 to 0.125
- down_weight: bfloat16 [16, 7168, 2048], P('ep', 'tp'), may hold values from -0.0625 to 0.0625
- output_gain: float32 [2048], replicated, may hold values from 0.1 to 1.9
Outputs:
- attended: bfloat16 [16384, 1024], P('ep', 'tp')
- moe_output: bfloat16 [12288, 2048], P(('ep', 'tp'))
Inputs may be any that keep to these rules, and one draw needn't show every extreme that they name: `expert_ids`: the 2 experts of a token differ. In the rows of one device (aligned blocks of 48 tokens) no expert is named by more than 7 tokens, and in every draw some expert is named by exactly 7 tokens of some device.
All inputs are finite; a program needn't handle non-finite values.
Results may differ from a plain program's by a relative error of at most 0.0085.
The roundings to bfloat16 on the way count: a program that leaves them out, or rounds other values in their place, can miss the bound.
Values may be sent and summed in bfloat16 or wider, within the bound.
A program may use at most 128 MiB of HBM per device.

v0:
```python
import math
import jax
import jax.numpy as jnp
from jax import lax
from jax.sharding import Mesh
from jax.sharding import PartitionSpec as P

QH = 16
KV = 4
GRID_W = 64
TP = ("tp_0", "tp_1")
EP_TP = ("ep", "tp_0", "tp_1")
rope_theta = 10000.0
rms_epsilon = 1e-06
norm_epsilon = 1e-05
residual_scale = 1.4142135623730951


def side_by_side(arrays, axis, dim, along):
    ends, at = ([], 0)
    for a in arrays[:-1]:
        at += a.shape[along]
        ends.append(at)
    both = jnp.concatenate(arrays, axis=along)
    return tuple(jnp.split(lax.all_gather(both, axis, axis=dim, tiled=True), ends, axis=along))


def sum_by_axis(terms, axes):
    subtotal = terms.astype(jnp.bfloat16)
    for axis in axes:
        subtotal = lax.psum_scatter(subtotal, axis, scatter_dimension=0, tiled=True)
    return subtotal.astype(jnp.float32)


def unit_heads(heads, gain_vector):
    squares = jnp.mean(heads * heads, axis=-1, keepdims=True)
    return heads * lax.rsqrt(squares + rms_epsilon) * gain_vector


def rotate_grid(heads, first_position, grid_width):
    head_size = heads.shape[-1]
    pair_count = head_size // 4
    position = first_position + jnp.arange(heads.shape[1], dtype=jnp.int32)
    grid_row = (position // grid_width).astype(jnp.float32)
    grid_col = (position % grid_width).astype(jnp.float32)
    inverse = rope_theta ** (-jnp.arange(pair_count, dtype=jnp.float32) / pair_count)
    angles = jnp.concatenate([grid_row[:, None] * inverse, grid_col[:, None] * inverse], axis=-1)
    cosines = jnp.cos(angles)
    sines = jnp.sin(angles)
    half_size = head_size // 2
    first_half = heads[..., :half_size]
    second_half = heads[..., half_size:]
    return jnp.concatenate(
        [first_half * cosines - second_half * sines, second_half * cosines + first_half * sines],
        axis=-1,
    )


def place_rank(choices, expert_count):
    matches = (choices[..., None] == jnp.arange(expert_count, dtype=jnp.int32)).astype(jnp.int32)
    earlier = jnp.cumsum(matches, axis=1) - matches
    return jnp.sum(earlier * matches, axis=-1)


def shards(
    queries,
    keys,
    values,
    query_gain,
    key_gain,
    moe_input,
    expert_ids,
    route_weight,
    gate_weight,
    up_weight,
    down_weight,
    output_gain,
):
    seg_rows = queries.shape[0]
    head_size = query_gain.shape[0]
    local_heads = queries.shape[1] // head_size
    offset = lax.axis_index("ep") * seg_rows
    key_head = lax.axis_index(TP) * local_heads // (QH // KV)
    key_cols = lax.dynamic_slice_in_dim(keys, key_head * head_size, head_size, 1)
    value_cols = lax.dynamic_slice_in_dim(values, key_head * head_size, head_size, 1)
    query_heads = (
        queries.reshape(seg_rows, local_heads, head_size).transpose(1, 0, 2).astype(jnp.float32)
    )
    rotated_queries = rotate_grid(unit_heads(query_heads, query_gain), offset, GRID_W).astype(
        jnp.bfloat16
    )
    key_heads = key_cols.astype(jnp.float32)[None]
    rotated_keys = rotate_grid(unit_heads(key_heads, key_gain), offset, GRID_W)[0].astype(
        jnp.bfloat16
    )
    score_scale = head_size ** (-0.5)
    initial = (
        jnp.full((local_heads, seg_rows), -jnp.inf, jnp.float32),
        jnp.zeros((local_heads, seg_rows), jnp.float32),
        jnp.zeros((local_heads, head_size, seg_rows), jnp.float32),
    )
    key_piece, value_piece = side_by_side((rotated_keys, value_cols), "ep", 0, 1)
    piece_rows = key_piece.shape[0]
    block_rows = math.gcd(piece_rows, 1024)
    key_blocks = key_piece.reshape(piece_rows // block_rows, block_rows, head_size)
    value_blocks = value_piece.reshape(piece_rows // block_rows, block_rows, head_size)

    def sweep(state_now, blocks):
        running_max, row_total, summed = state_now
        key_block, value_block = blocks
        scores = (
            jnp.einsum(
                "hqd,kd->hqk", rotated_queries, key_block, preferred_element_type=jnp.float32
            )
            * score_scale
        )
        new_max = jnp.maximum(running_max, jnp.max(scores, axis=-1))
        shrink = jnp.exp(running_max - new_max)
        weights = jnp.exp(scores - new_max[..., None])
        row_total = row_total * shrink + jnp.sum(weights, axis=-1)
        added = jnp.einsum(
            "hqk,kd->hdq",
            weights.astype(jnp.bfloat16),
            value_block,
            preferred_element_type=jnp.float32,
        )
        summed = summed * shrink[:, None, :] + added
        return ((new_max, row_total, summed), None)

    result, ignored = lax.scan(sweep, initial, (key_blocks, value_blocks))
    row_max, row_total, summed = result
    attended = (
        (summed / row_total[:, None, :])
        .transpose(2, 0, 1)
        .reshape(seg_rows, local_heads * head_size)
        .astype(jnp.bfloat16)
    )
    tok_rows = moe_input.shape[0]
    model_width = moe_input.shape[1]
    top_count = expert_ids.shape[1]
    experts = lax.axis_size("ep")
    capacity = max(2, tok_rows * top_count * 5 // (4 * experts))
    column_index = lax.axis_index(TP)
    own_ids = lax.dynamic_slice_in_dim(expert_ids, column_index * tok_rows, tok_rows, 0).reshape(-1)
    own_weights = lax.dynamic_slice_in_dim(route_weight, column_index * tok_rows, tok_rows, 0)
    own_rank = place_rank(own_ids[None], experts)[0]
    own_slots = own_ids * capacity + own_rank
    token_of = jnp.arange(tok_rows * top_count, dtype=jnp.int32) // top_count
    sources = jnp.full((experts * capacity,), tok_rows, jnp.int32).at[own_slots].set(token_of)
    outgoing = jnp.take(moe_input, sources, axis=0, mode="fill", fill_value=0)
    arrived = lax.all_to_all(
        outgoing.reshape(experts, capacity, model_width),
        "ep",
        split_axis=0,
        concat_axis=0,
        tiled=True,
    )
    shard_piece = lax.all_gather(arrived.reshape(-1, model_width), TP, axis=0, tiled=True)
    gate_part = jnp.dot(shard_piece, gate_weight[0], preferred_element_type=jnp.float32)
    up_part = jnp.dot(shard_piece, up_weight[0], preferred_element_type=jnp.float32)
    hidden = (jax.nn.silu(gate_part) * up_part).astype(jnp.bfloat16)
    expert_out = sum_by_axis(
        jnp.dot(hidden, down_weight[0], preferred_element_type=jnp.float32), TP
    ).astype(jnp.bfloat16)
    returned = lax.all_to_all(
        expert_out.reshape(experts, capacity, model_width),
        "ep",
        split_axis=0,
        concat_axis=0,
        tiled=True,
    )
    picked = jnp.take(returned.reshape(experts * capacity, model_width), own_slots, axis=0)
    picked = picked.reshape(tok_rows, top_count, model_width).astype(jnp.float32)
    mixed = residual_scale * moe_input.astype(jnp.float32) + jnp.sum(
        own_weights[:, :, None] * picked, axis=1
    )
    average = jnp.mean(mixed, axis=-1, keepdims=True)
    centered = mixed - average
    variance = jnp.mean(centered * centered, axis=-1, keepdims=True)
    moe_output = (centered * lax.rsqrt(variance + norm_epsilon) * output_gain).astype(jnp.bfloat16)
    return (attended, moe_output)


def solution(mesh):
    split = Mesh(mesh.devices.reshape(mesh.shape["ep"], 8, 2), ("ep", "tp_0", "tp_1"))
    return jax.shard_map(
        shards,
        mesh=split,
        in_specs=(
            P("ep", TP),
            P("ep", None),
            P("ep", None),
            P(),
            P(),
            P(EP_TP, None),
            P("ep", None),
            P("ep", None),
            P("ep", None, TP),
            P("ep", None, TP),
            P("ep", TP, None),
            P(),
        ),
        out_specs=(P("ep", TP), P(EP_TP, None)),
        check_vma=False,
    )
```

profile of v0, /device:TPU:1, one launch (start us, length us, event | category | flops | bytes accessed | tf_op | source)
XLA Modules:
  0.0 365.4 jit_solution(13836861877901142481)
XLA Ops:
  10.7 2.3 gather_fusion
  13.4 17.8 %all_to_all.10 = bf16[16,7,2048]{2,1,0:T(8,128)(2,1)S(1)} all-to-all(bf16[16,7,2048]{2,1,0:T(8,128)(2,1)S(1)} %broadcast_select_fusion.3), channel_id=1, replica_groups=mesh['ep'=16,'tp_0'=8,'tp_1'=2] {'ep'}, dimensions={0} | all-to-all | bytes 917504 | tf_op jit(solution)/shard_map/all_to_all | solution.py:151
  32.2 51.9 %all-gather.5.cloned.1.call-done = bf16[1792,2048]{1,0:T(8,128)(2,1)} async-done(((bf16[112,2048]{1,0:T(8,128)(2,1)}), bf16[1792,2048]{1,0:T(8,128)(2,1)}) %all-gather.5.cloned.1.call-update) | async-done | bytes 7340048 | tf_op jit(solution)/shard_map/all_gather | solution.py:158
  84.1 7.3 %fusion.24 = f32[1792,448]{0,1:T(8,128)S(1)} fusion(bf16[1792,2048]{1,0:T(8,128)(2,1)} %all-gather.5.cloned.1.call-done, bf16[1,2048,448]{1,2,0:T(8,128)(2,1)} %param.22), kind=kOutput, calls=%fused_computation.30 | convolution fusion | flops 3288334336 | bytes 12386304 | tf_op jit(solution)/shard_map/dot_general | solution.py:159
  91.4 3.8 %multiply_convert_fusion = bf16[1792,448]{0,1:T(8,128)(2,1)S(1)} fusion(f32[1792,448]{0,1:T(8,128)S(1)} %fusion.24, bf16[1792,2048]{1,0:T(8,128)(2,1)S(1)} %copy-done.8, bf16[1,2048,448]{1,2,0:T(8,128)(2,1)S(1)} %copy-done.9), kind=kOutput, calls=%fused_computation.27 | convolution fusion | flops 3293151232 | bytes 13991936 | tf_op jit(solution)/shard_map/dot_general | solution.py:160
  95.1 6.1 %convolution_convert_fusion = bf16[1792,2048]{1,0:T(8,128)(2,1)} fusion(bf16[1792,448]{0,1:T(8,128)(2,1)S(1)} %multiply_convert_fusion, bf16[1,448,2048]{2,1,0:T(8,128)(2,1)S(1)} %copy-done), kind=kOutput, calls=%fused_computation.26 | convolution fusion | flops 3292004352 | bytes 10780672 | tf_op jit(solution)/shard_map/dot_general | solution.py:163
  102.3 1.2 constant_dynamic-slice_fusion.2
  107.2 77.4 %reduce-scatter.3.cloned.1.call-done = bf16[224,2048]{1,0:T(8,128)(2,1)} async-done(((bf16[1792,2048]{1,0:T(8,128)(2,1)}), bf16[224,2048]{1,0:T(8,128)(2,1)}) %reduce-scatter.3.cloned.1.call-update) | async-done | bytes 917520 | tf_op jit(solution)/shard_map/reduce_scatter | solution.py:31
  184.7 4.7 %fusion.47 = (bf16[16384,64]{0,1:T(8,128)(2,1)}, bf16[16384,64]{0,1:T(8,128)(2,1)}) fusion(bf16[16384,128]{0,1:T(8,128)(2,1)} %all-gather.3.cloned.1.call-done), kind=kLoop, calls=%fused_computation.105 | loop fusion | bytes 8388608 | tf_op jit(solution)/shard_map/split | solution.py:25
  189.3 4.8 %copy.37 = bf16[16384,64]{1,0:T(8,128)(2,1)} copy(bf16[16384,64]{0,1:T(8,128)(2,1)} %get-tuple-element.101) | data formatting | bytes 4194304
  194.1 5.0 %copy.38 = bf16[16384,64]{1,0:T(8,128)(2,1)} copy(bf16[16384,64]{0,1:T(8,128)(2,1)} %get-tuple-element.100) | data formatting | bytes 4194304
  199.1 1.1 reduce-scatter.5.cloned.1.call-done
  200.2 2.0 reshape.467
  202.1 6.2 %all-to-all-start.1 = ((bf16[16,7,2048]{2,1,0:T(8,128)(2,1)}), bf16[16,7,2048]{2,1,0:T(8,128)(2,1)S(1)}, u32[]{:S(2)}, u32[]{:S(2)}) async-start(bf16[16,7,2048]{2,1,0:T(8,128)(2,1)} %reshape.467), calls=%async_computation.3 | async-start | bytes 1048576 | tf_op jit(solution)/shard_map/all_to_all | solution.py:165
  208.4 144.6 %while.15 = (s32[]{:T(128)}, f32[1,1024]{1,0:T(1,128)S(1)}, f32[1,1024]{1,0:T(1,128)S(1)}, f32[1,64,1024]{2,1,0:T(8,128)S(1)}, bf16[16,1024,64]{2,1,0:T(8,128)(2...) while((s32[]{:T(128)}, f32[1,1024]{1,0:T(1,128)S(1)}, ...), condition=%wide.region_5.6_spmd.clone, body=%wide.region_2.5_spmd.clone.sunk | while | flops 277025792 | bytes 30605460 | solution.py:130
  208.4 3.8 %multiply_reduce_fusion.4 = (f32[1024]{0:T(1024)S(1)}, f32[1024,1024]{1,0:T(8,128)}) fusion(bf16[1,1024,64]{2,1,0:T(8,128)(2,1)S(1)} %get-tuple-element.188, bf16[16,1024,64]{2,1,0:T(8,128)(2,1)} %get-tuple-element.187, s32[]{:T(128)S(6)} %copy.45), kind=kOutput, calls=%fused_computation.4.clone.1 | convolution fusion | flops 136313856 | bytes 4591620 | tf_op jit(solution)/shard_map/while/body/eval_jaxpr/hqd,kd->hqk/dot_general | solution.py:112
  212.2 3.1 fusion.60
  215.6 1.8 fusion.62
  217.4 3.8 %multiply_reduce_fusion.4 = (f32[1024]{0:T(1024)S(1)}, f32[1024,1024]{1,0:T(8,128)}) fusion(bf16[1,1024,64]{2,1,0:T(8,128)(2,1)S(1)} %get-tuple-element.188, bf16[16,1024,64]{2,1,0:T(8,128)(2,1)} %get-tuple-element.187, s32[]{:T(128)S(6)} %copy.45), kind=kOutput, calls=%fused_computation.4.clone.1 | convolution fusion | flops 136313856 | bytes 4591620 | tf_op jit(solution)/shard_map/while/body/eval_jaxpr/hqd,kd->hqk/dot_general | solution.py:112
  221.2 3.1 fusion.60
  224.7 1.8 fusion.62
  226.5 3.8 %multiply_reduce_fusion.4 = (f32[1024]{0:T(1024)S(1)}, f32[1024,1024]{1,0:T(8,128)}) fusion(bf16[1,1024,64]{2,1,0:T(8,128)(2,1)S(1)} %get-tuple-element.188, bf16[16,1024,64]{2,1,0:T(8,128)(2,1)} %get-tuple-element.187, s32[]{:T(128)S(6)} %copy.45), kind=kOutput, calls=%fused_computation.4.clone.1 | convolution fusion | flops 136313856 | bytes 4591620 | tf_op jit(solution)/shard_map/while/body/eval_jaxpr/hqd,kd->hqk/dot_general | solution.py:112
  230.3 3.1 fusion.60
  233.7 1.8 fusion.62
  235.5 3.8 %multiply_reduce_fusion.4 = (f32[1024]{0:T(1024)S(1)}, f32[1024,1024]{1,0:T(8,128)}) fusion(bf16[1,1024,64]{2,1,0:T(8,128)(2,1)S(1)} %get-tuple-element.188, bf16[16,1024,64]{2,1,0:T(8,128)(2,1)} %get-tuple-element.187, s32[]{:T(128)S(6)} %copy.45), kind=kOutput, calls=%fused_computation.4.clone.1 | convolution fusion | flops 136313856 | bytes 4591620 | tf_op jit(solution)/shard_map/while/body/eval_jaxpr/hqd,kd->hqk/dot_general | solution.py:112
  239.3 3.1 fusion.60
  242.7 1.8 fusion.62
  244.5 3.8 %multiply_reduce_fusion.4 = (f32[1024]{0:T(1024)S(1)}, f32[1024,1024]{1,0:T(8,128)}) fusion(bf16[1,1024,64]{2,1,0:T(8,128)(2,1)S(1)} %get-tuple-element.188, bf16[16,1024,64]{2,1,0:T(8,128)(2,1)} %get-tuple-element.187, s32[]{:T(128)S(6)} %copy.45), kind=kOutput, calls=%fused_computation.4.clone.1 | convolution fusion | flops 136313856 | bytes 4591620 | tf_op jit(solution)/shard_map/while/body/eval_jaxpr/hqd,kd->hqk/dot_general | solution.py:112
  248.3 3.1 fusion.60
  251.8 1.8 fusion.62
  253.6 3.8 %multiply_reduce_fusion.4 = (f32[1024]{0:T(1024)S(1)}, f32[1024,1024]{1,0:T(8,128)}) fusion(bf16[1,1024,64]{2,1,0:T(8,128)(2,1)S(1)} %get-tuple-element.188, bf16[16,1024,64]{2,1,0:T(8,128)(2,1)} %get-tuple-element.187, s32[]{:T(128)S(6)} %copy.45), kind=kOutput, calls=%fused_computation.4.clone.1 | convolution fusion | flops 136313856 | bytes 4591620 | tf_op jit(solution)/shard_map/while/body/eval_jaxpr/hqd,kd->hqk/dot_general | solution.py:112
  257.4 3.1 fusion.60
  260.8 1.8 fusion.62
  262.6 3.8 %multiply_reduce_fusion.4 = (f32[1024]{0:T(1024)S(1)}, f32[1024,1024]{1,0:T(8,128)}) fusion(bf16[1,1024,64]{2,1,0:T(8,128)(2,1)S(1)} %get-tuple-element.188, bf16[16,1024,64]{2,1,0:T(8,128)(2,1)} %get-tuple-element.187, s32[]{:T(128)S(6)} %copy.45), kind=kOutput, calls=%fused_computation.4.clone.1 | convolution fusion | flops 136313856 | bytes 4591620 | tf_op jit(solution)/shard_map/while/body/eval_jaxpr/hqd,kd->hqk/dot_general | solution.py:112
  266.4 3.1 fusion.60
  269.8 1.8 fusion.62
  271.7 3.8 %multiply_reduce_fusion.4 = (f32[1024]{0:T(1024)S(1)}, f32[1024,1024]{1,0:T(8,128)}) fusion(bf16[1,1024,64]{2,1,0:T(8,128)(2,1)S(1)} %get-tuple-element.188, bf16[16,1024,64]{2,1,0:T(8,128)(2,1)} %get-tuple-element.187, s32[]{:T(128)S(6)} %copy.45), kind=kOutput, calls=%fused_computation.4.clone.1 | convolution fusion | flops 136313856 | bytes 4591620 | tf_op jit(solution)/shard_map/while/body/eval_jaxpr/hqd,kd->hqk/dot_general | solution.py:112
  275.4 3.1 fusion.60
  278.9 1.8 fusion.62
  280.7 3.8 %multiply_reduce_fusion.4 = (f32[1024]{0:T(1024)S(1)}, f32[1024,1024]{1,0:T(8,128)}) fusion(bf16[1,1024,64]{2,1,0:T(8,128)(2,1)S(1)} %get-tuple-element.188, bf16[16,1024,64]{2,1,0:T(8,128)(2,1)} %get-tuple-element.187, s32[]{:T(128)S(6)} %copy.45), kind=kOutput, calls=%fused_computation.4.clone.1 | convolution fusion | flops 136313856 | bytes 4591620 | tf_op jit(solution)/shard_map/while/body/eval_jaxpr/hqd,kd->hqk/dot_general | solution.py:112
  284.5 3.1 fusion.60
  287.9 1.8 fusion.62
  289.7 3.8 %multiply_reduce_fusion.4 = (f32[1024]{0:T(1024)S(1)}, f32[1024,1024]{1,0:T(8,128)}) fusion(bf16[1,1024,64]{2,1,0:T(8,128)(2,1)S(1)} %get-tuple-element.188, bf16[16,1024,64]{2,1,0:T(8,128)(2,1)} %get-tuple-element.187, s32[]{:T(128)S(6)} %copy.45), kind=kOutput, calls=%fused_computation.4.clone.1 | convolution fusion | flops 136313856 | bytes 4591620 | tf_op jit(solution)/shard_map/while/body/eval_jaxpr/hqd,kd->hqk/dot_general | solution.py:112
  293.5 3.1 fusion.60
  296.9 1.8 fusion.62
  298.8 3.8 %multiply_reduce_fusion.4 = (f32[1024]{0:T(1024)S(1)}, f32[1024,1024]{1,0:T(8,128)}) fusion(bf16[1,1024,64]{2,1,0:T(8,128)(2,1)S(1)} %get-tuple-element.188, bf16[16,1024,64]{2,1,0:T(8,128)(2,1)} %get-tuple-element.187, s32[]{:T(128)S(6)} %copy.45), kind=kOutput, calls=%fused_computation.4.clone.1 | convolution fusion | flops 136313856 | bytes 4591620 | tf_op jit(solution)/shard_map/while/body/eval_jaxpr/hqd,kd->hqk/dot_general | solution.py:112
  302.5 3.1 fusion.60
  306.0 1.8 fusion.62
  307.8 3.8 %multiply_reduce_fusion.4 = (f32[1024]{0:T(1024)S(1)}, f32[1024,1024]{1,0:T(8,128)}) fusion(bf16[1,1024,64]{2,1,0:T(8,128)(2,1)S(1)} %get-tuple-element.188, bf16[16,1024,64]{2,1,0:T(8,128)(2,1)} %get-tuple-element.187, s32[]{:T(128)S(6)} %copy.45), kind=kOutput, calls=%fused_computation.4.clone.1 | convolution fusion | flops 136313856 | bytes 4591620 | tf_op jit(solution)/shard_map/while/body/eval_jaxpr/hqd,kd->hqk/dot_general | solution.py:112
  311.6 3.1 fusion.60
  315.0 1.8 fusion.62
  316.8 3.8 %multiply_reduce_fusion.4 = (f32[1024]{0:T(1024)S(1)}, f32[1024,1024]{1,0:T(8,128)}) fusion(bf16[1,1024,64]{2,1,0:T(8,128)(2,1)S(1)} %get-tuple-element.188, bf16[16,1024,64]{2,1,0:T(8,128)(2,1)} %get-tuple-element.187, s32[]{:T(128)S(6)} %copy.45), kind=kOutput, calls=%fused_computation.4.clone.1 | convolution fusion | flops 136313856 | bytes 4591620 | tf_op jit(solution)/shard_map/while/body/eval_jaxpr/hqd,kd->hqk/dot_general | solution.py:112
  320.6 3.1 fusion.60
  324.0 1.8 fusion.62
  325.9 3.8 %multiply_reduce_fusion.4 = (f32[1024]{0:T(1024)S(1)}, f32[1024,1024]{1,0:T(8,128)}) fusion(bf16[1,1024,64]{2,1,0:T(8,128)(2,1)S(1)} %get-tuple-element.188, bf16[16,1024,64]{2,1,0:T(8,128)(2,1)} %get-tuple-element.187, s32[]{:T(128)S(6)} %copy.45), kind=kOutput, calls=%fused_computation.4.clone.1 | convolution fusion | flops 136313856 | bytes 4591620 | tf_op jit(solution)/shard_map/while/body/eval_jaxpr/hqd,kd->hqk/dot_general | solution.py:112
  329.6 3.1 fusion.60
  333.1 1.8 fusion.62
  334.9 3.8 %multiply_reduce_fusion.4 = (f32[1024]{0:T(1024)S(1)}, f32[1024,1024]{1,0:T(8,128)}) fusion(bf16[1,1024,64]{2,1,0:T(8,128)(2,1)S(1)} %get-tuple-element.188, bf16[16,1024,64]{2,1,0:T(8,128)(2,1)} %get-tuple-element.187, s32[]{:T(128)S(6)} %copy.45), kind=kOutput, calls=%fused_computation.4.clone.1 | convolution fusion | flops 136313856 | bytes 4591620 | tf_op jit(solution)/shard_map/while/body/eval_jaxpr/hqd,kd->hqk/dot_general | solution.py:112
  338.7 3.1 fusion.60
  342.1 1.8 fusion.62
  343.9 3.8 %multiply_reduce_fusion.4 = (f32[1024]{0:T(1024)S(1)}, f32[1024,1024]{1,0:T(8,128)}) fusion(bf16[1,1024,64]{2,1,0:T(8,128)(2,1)S(1)} %get-tuple-element.188, bf16[16,1024,64]{2,1,0:T(8,128)(2,1)} %get-tuple-element.187, s32[]{:T(128)S(6)} %copy.45), kind=kOutput, calls=%fused_computation.4.clone.1 | convolution fusion | flops 136313856 | bytes 4591620 | tf_op jit(solution)/shard_map/while/body/eval_jaxpr/hqd,kd->hqk/dot_general | solution.py:112
  347.7 3.1 fusion.60
  351.2 1.8 fusion.62
  354.9 2.0 multiply_reduce_fusion.1
  (161 shorter events, 17.5 us)
Async XLA Ops:
  8.0 87.1 %copy-start = (bf16[1,448,2048]{2,1,0:T(8,128)(2,1)S(1)}, bf16[1,448,2048]{2,1,0:T(8,128)(2,1)}, u32[]{:S(2)}) copy-start(bf16[1,448,2048]{2,1,0:T(8,128)(2,1)} %param.24) | copy-start | bytes 5505028
  8.0 76.1 %all-gather.5.cloned.1.call-start = ((), (), s32[]{:S(2)}) async-start(), calls=%async_computation.5 | async-start | bytes 7798784 | tf_op jit(solution)/shard_map/all_gather | solution.py:158
  32.1 152.5 %reduce-scatter.3.cloned.1.call-start = ((), (), s32[]{:S(2)}) async-start(), calls=%async_computation.6 | async-start | bytes 8257536 | tf_op jit(solution)/shard_map/reduce_scatter | solution.py:31
  84.1 7.3 %copy-start.8 = (bf16[1792,2048]{1,0:T(8,128)(2,1)S(1)}, bf16[1792,2048]{1,0:T(8,128)(2,1)}, u32[]{:S(2)}) copy-start(bf16[1792,2048]{1,0:T(8,128)(2,1)} %all-gather.5.cloned.1.call-done) | copy-start | bytes 22020100
  84.1 7.3 %copy-start.9 = (bf16[1,2048,448]{1,2,0:T(8,128)(2,1)S(1)}, bf16[1,2048,448]{1,2,0:T(8,128)(2,1)}, u32[]{:S(2)}) copy-start(bf16[1,2048,448]{1,2,0:T(8,128)(2,1)} %param.23) | copy-start | bytes 5505028
  101.3 1.0 copy-start.4
  101.3 2.5 copy-start.3
  101.3 2.7 copy-start.6
  101.3 2.8 copy-start.7
  101.3 83.3 %all-gather.3.cloned.1.call-start = ((), (), s32[]{:S(2)}) async-start(), calls=%async_computation.4 | async-start | bytes 4456448 | tf_op jit(solution)/shard_map/all_gather | solution.py:25
  105.5 94.7 %reduce-scatter.5.cloned.1.call-start = ((), (), s32[]{:S(2)}) async-start(), calls=%async_computation.7 | async-start | bytes 1376256 | tf_op jit(solution)/shard_map/reduce_scatter | solution.py:31
  202.1 151.5 %all-to-all-start.1 = ((bf16[16,7,2048]{2,1,0:T(8,128)(2,1)}), bf16[16,7,2048]{2,1,0:T(8,128)(2,1)S(1)}, u32[]{:S(2)}, u32[]{:S(2)}) async-start(bf16[16,7,2048]{2,1,0:T(8,128)(2,1)} %reshape.467), calls=%async_computation.3 | async-start | bytes 1048576 | tf_op jit(solution)/shard_map/all_to_all | solution.py:165
  212.2 3.4 copy-start.1
  221.2 3.4 copy-start.1
  230.2 3.4 copy-start.1
  239.3 3.4 copy-start.1
  248.3 3.4 copy-start.1
  257.3 3.4 copy-start.1
  266.4 3.4 copy-start.1
  275.4 3.4 copy-start.1
  284.5 3.4 copy-start.1
  293.5 3.4 copy-start.1
  302.5 3.4 copy-start.1
  311.6 3.4 copy-start.1
  320.6 3.4 copy-start.1
  329.6 3.4 copy-start.1
  338.7 3.4 copy-start.1
  347.7 3.4 copy-start.1
  353.0 4.0 %copy-start.2 = (bf16[48,2048]{1,0:T(8,128)(2,1)S(1)}, bf16[48,2048]{1,0:T(8,128)(2,1)}, u32[]{:S(2)}) copy-start(bf16[48,2048]{1,0:T(8,128)(2,1)} %param.19) | copy-start | bytes 589828
  353.0 4.4 %copy-start.5 = (f32[2048]{0:T(1024)S(1)}, f32[2048]{0:T(1024)}, u32[]{:S(2)}) copy-start(f32[2048]{0:T(1024)} %param.25) | copy-start | bytes 24580
Sparse Core Ops, SparseCore 0:
  32.3 51.7 all-gather.4
  101.4 83.1 reduce-scatter.2
  187.1 13.0 reduce-scatter.4
Sparse Core Ops, SparseCore 1:
  105.6 54.1 all-gather.2
where the time goes:
time: 367 us; the launch traced here: 365 us
  waiting for transfers between devices  130 us (35%)
  matrix products  106 us (29%)
  other arithmetic  56.6 us (15%)
  local copies, waits for them, and re-layouts  31.5 us (9%)
  blocking collectives  17.8 us (5%)
  between operations  15.6 us (4%)
  starting transfers between devices  6.59 us (2%)
    reduce_scatter x2, waiting for transfers between devices, sum_by_axis(): subtotal = lax.psum_scatter(subtotal, axis, scatter_dimension=0, tiled=True)  78.5 us
    dot_general x16, matrix products, sweep(): jnp.einsum('hqd,kd->hqk', rotated_queries, key_block, preferred_element_t...  60.3 us
    all_gather x1, waiting for transfers between devices, shards(): lax.all_gather(arrived.reshape(-1, model_width), TP, axis=0, tiled=True)  51.9 us
    reduce_sum x16, other arithmetic, sweep(): row_total = row_total * shrink + jnp.sum(weights, axis=-1)  49.1 us
    dot_general x16, matrix products, sweep(): jnp.einsum('hqk,kd->hdq', weights.astype(jnp.bfloat16), value_block, pref...  28.8 us
    all_to_all x1, blocking collectives, shards(): lax.all_to_all(outgoing.reshape(experts, capacity, model_width), 'ep', sp...  17.8 us
    unnamed x23, local copies, waits for them, and re-layouts  11.2 us
  transfers between devices with their start and end apart: 5, of which 3 were waited for; matrix products, arithmetic and copies ran while one was open for 43% of the time, Pallas kernels for 0%

commit v1 on v0

--- a/solution.py
+++ b/solution.py
@@ -155,7 +155,10 @@
         concat_axis=0,
         tiled=True,
     )
-    shard_piece = lax.all_gather(arrived.reshape(-1, model_width), TP, axis=0, tiled=True)
+    shard_piece = jnp.concatenate(
+        lax.all_to_all(jnp.stack([arrived.reshape(-1, model_width)] * lax.axis_size(TP)), TP, 0, 0),
+        axis=0,
+    )
     gate_part = jnp.dot(shard_piece, gate_weight[0], preferred_element_type=jnp.float32)
     up_part = jnp.dot(shard_piece, up_weight[0], preferred_element_type=jnp.float32)
     hidden = (jax.nn.silu(gate_part) * up_part).astype(jnp.bfloat16)

time: 367 us -> 480 us (1.31)
  blocking collectives: 17.8 us -> 192 us
  waiting for transfers between devices: 130 us -> 73.6 us
    all_to_all x0 -> x1, blocking collectives: none -> 174 us  [shards(): lax.all_to_all(jnp.stack([arrived.reshape(-1, model_width)] * lax.axis_si...]
    all_gather x1 -> x0, waiting for transfers between devices: 51.9 us -> none  [shards(): lax.all_gather(arrived.reshape(-1, model_width), TP, axis=0, tiled=True)]
    reduce_scatter x2, waiting for transfers between devices: 78.5 us -> 73.5 us  [sum_by_axis(): subtotal = lax.psum_scatter(subtotal, axis, scatter_dimension=0, tiled=True)]
  transfers between devices with their start and end apart: 5 -> 4, of which waited for: 3 -> 2; matrix products, arithmetic and copies ran while one was open for 43% -> 33% of each run, Pallas kernels for 0% -> 0%
where the time goes in v1:
time: 480 us; the launch traced here: 479 us
  blocking collectives  192 us (40%)
  matrix products  102 us (21%)
  waiting for transfers between devices  73.6 us (15%)
  other arithmetic  56.6 us (12%)
  local copies, waits for them, and re-layouts  31.6 us (7%)
  between operations  15.9 us (3%)
  starting transfers between devices  6.56 us (1%)
    all_to_all x1, blocking collectives, shards(): lax.all_to_all(jnp.stack([arrived.reshape(-1, model_width)] * lax.axis_si...  174 us
    reduce_scatter x2, waiting for transfers between devices, sum_by_axis(): subtotal = lax.psum_scatter(subtotal, axis, scatter_dimension=0, tiled=True)  73.5 us
    dot_general x16, matrix products, sweep(): jnp.einsum('hqd,kd->hqk', rotated_queries, key_block, preferred_element_t...  60.3 us
    reduce_sum x16, other arithmetic, sweep(): row_total = row_total * shrink + jnp.sum(weights, axis=-1)  49.1 us
    dot_general x16, matrix products, sweep(): jnp.einsum('hqk,kd->hdq', weights.astype(jnp.bfloat16), value_block, pref...  28.8 us
    all_to_all x1, blocking collectives, shards(): lax.all_to_all(outgoing.reshape(experts, capacity, model_width), 'ep', sp...  17.8 us
    unnamed x23, local copies, waits for them, and re-layouts  11 us
  transfers between devices with their start and end apart: 4, of which 2 were waited for; matrix products, arithmetic and copies ran while one was open for 33% of the time, Pallas kernels for 0%

profile of v1, /device:TPU:1, one launch (start us, length us, event | category | flops | bytes accessed | tf_op | source)
XLA Modules:
  0.0 478.9 jit_solution(5194624725411069759)
XLA Ops:
  10.7 2.3 gather_fusion
  13.4 17.8 %all_to_all.15 = bf16[16,7,2048]{2,1,0:T(8,128)(2,1)S(1)} all-to-all(bf16[16,7,2048]{2,1,0:T(8,128)(2,1)S(1)} %broadcast_select_fusion.3), channel_id=1, replica_groups=mesh['ep'=16,'tp_0'=8,'tp_1'=2] {'ep'}, dimensions={0} | all-to-all | bytes 917504 | tf_op jit(solution)/shard_map/all_to_all | solution.py:151
  32.3 173.7 %all_to_all.16 = bf16[16,112,2048]{2,1,0:T(8,128)(2,1)S(1)} all-to-all(bf16[16,112,2048]{2,1,0:T(8,128)(2,1)S(1)} %stack.3), channel_id=1, replica_groups=mesh['ep'=16,'tp_0'=8,'tp_1'=2] {'tp_0','tp_1'}, dimensions={0} | all-to-all | bytes 14680064 | tf_op jit(solution)/shard_map/all_to_all | solution.py:159
  206.0 3.5 fusion.24
  209.6 3.8 multiply_convert_fusion
  213.4 6.1 %convolution_convert_fusion = bf16[1792,2048]{1,0:T(8,128)(2,1)} fusion(bf16[1792,448]{0,1:T(8,128)(2,1)S(1)} %multiply_convert_fusion, bf16[1,448,2048]{2,1,0:T(8,128)(2,1)S(1)} %copy-done), kind=kOutput, calls=%fused_computation.26 | convolution fusion | flops 3292004352 | bytes 10780672 | tf_op jit(solution)/shard_map/dot_general | solution.py:166
  220.5 1.2 constant_dynamic-slice_fusion.2
  225.2 72.4 %reduce-scatter.3.cloned.1.call-done = bf16[224,2048]{1,0:T(8,128)(2,1)} async-done(((bf16[1792,2048]{1,0:T(8,128)(2,1)}), bf16[224,2048]{1,0:T(8,128)(2,1)}) %reduce-scatter.3.cloned.1.call-update) | async-done | bytes 917520 | tf_op jit(solution)/shard_map/reduce_scatter | solution.py:31
  297.6 4.7 fusion.47
  302.3 4.8 copy.37
  307.1 5.0 %copy.38 = bf16[16384,64]{1,0:T(8,128)(2,1)} copy(bf16[16384,64]{0,1:T(8,128)(2,1)} %get-tuple-element.100) | data formatting | bytes 4194304
  312.1 1.1 reduce-scatter.5.cloned.1.call-done
  313.2 2.0 reshape.469
  315.1 6.3 %all-to-all-start.2 = ((bf16[16,7,2048]{2,1,0:T(8,128)(2,1)}), bf16[16,7,2048]{2,1,0:T(8,128)(2,1)S(1)}, u32[]{:S(2)}, u32[]{:S(2)}) async-start(bf16[16,7,2048]{2,1,0:T(8,128)(2,1)} %reshape.469), calls=%async_computation.4 | async-start | bytes 1048576 | tf_op jit(solution)/shard_map/all_to_all | solution.py:168
  321.4 144.8 %while.15 = (s32[]{:T(128)}, f32[1,1024]{1,0:T(1,128)S(1)}, f32[1,1024]{1,0:T(1,128)S(1)}, f32[1,64,1024]{2,1,0:T(8,128)S(1)}, bf16[16,1024,64]{2,1,0:T(8,128)(2...) while((s32[]{:T(128)}, f32[1,1024]{1,0:T(1,128)S(1)}, ...), condition=%wide.region_5.6_spmd.clone, body=%wide.region_2.5_spmd.clone.sunk | while | flops 277025792 | bytes 30606468 | solution.py:130
  321.4 3.8 multiply_reduce_fusion.4
  325.2 3.1 fusion.60
  328.6 1.8 fusion.62
  330.5 3.8 multiply_reduce_fusion.4
  334.3 3.1 fusion.60
  337.7 1.8 fusion.62
  339.5 3.8 multiply_reduce_fusion.4
  343.3 3.1 fusion.60
  346.7 1.8 fusion.62
  348.6 3.8 multiply_reduce_fusion.4
  352.3 3.1 fusion.60
  355.8 1.8 fusion.62
  357.6 3.8 multiply_reduce_fusion.4
  361.4 3.1 fusion.60
  364.8 1.8 fusion.62
  366.7 3.8 multiply_reduce_fusion.4
  370.4 3.1 fusion.60
  373.9 1.8 fusion.62
  375.7 3.8 multiply_reduce_fusion.4
  379.5 3.1 fusion.60
  382.9 1.8 fusion.62
  384.8 3.8 multiply_reduce_fusion.4
  388.5 3.1 fusion.60
  392.0 1.8 fusion.62
  393.8 3.8 multiply_reduce_fusion.4
  397.6 3.1 fusion.60
  401.0 1.8 fusion.62
  402.9 3.8 multiply_reduce_fusion.4
  406.6 3.1 fusion.60
  410.1 1.8 fusion.62
  411.9 3.8 multiply_reduce_fusion.4
  415.7 3.1 fusion.60
  419.1 1.8 fusion.62
  421.0 3.8 multiply_reduce_fusion.4
  424.7 3.1 fusion.60
  428.2 1.8 fusion.62
  430.0 3.8 multiply_reduce_fusion.4
  433.8 3.1 fusion.60
  437.2 1.8 fusion.62
  439.1 3.8 multiply_reduce_fusion.4
  442.8 3.1 fusion.60
  446.3 1.8 fusion.62
  448.1 3.8 multiply_reduce_fusion.4
  451.9 3.1 fusion.60
  455.3 1.8 fusion.62
  457.2 3.8 multiply_reduce_fusion.4
  460.9 3.1 fusion.60
  464.4 1.8 fusion.62
  468.2 2.0 multiply_reduce_fusion.1
  (160 shorter events, 17.7 us)
Async XLA Ops:
  8.0 205.4 %copy-start = (bf16[1,448,2048]{2,1,0:T(8,128)(2,1)S(1)}, bf16[1,448,2048]{2,1,0:T(8,128)(2,1)}, u32[]{:S(2)}) copy-start(bf16[1,448,2048]{2,1,0:T(8,128)(2,1)} %param.24) | copy-start | bytes 5505028
  8.0 289.6 %reduce-scatter.3.cloned.1.call-start = ((), (), s32[]{:S(2)}) async-start(), calls=%async_computation.6 | async-start | bytes 8257536 | tf_op jit(solution)/shard_map/reduce_scatter | solution.py:31
  32.3 173.7 %copy-start.8 = (bf16[1,2048,448]{1,2,0:T(8,128)(2,1)S(1)}, bf16[1,2048,448]{1,2,0:T(8,128)(2,1)}, u32[]{:S(2)}) copy-start(bf16[1,2048,448]{1,2,0:T(8,128)(2,1)} %param.22) | copy-start | bytes 5505028
  206.0 3.5 copy-start.9
  219.5 1.0 copy-start.4
  219.5 2.6 copy-start.3
  219.5 2.7 copy-start.6
  219.5 2.8 copy-start.7
  219.5 78.1 %all-gather.2.cloned.1.call-start = ((), (), s32[]{:S(2)}) async-start(), calls=%async_computation.5 | async-start | bytes 4456448 | tf_op jit(solution)/shard_map/all_gather | solution.py:25
  223.7 89.4 %reduce-scatter.5.cloned.1.call-start = ((), (), s32[]{:S(2)}) async-start(), calls=%async_computation.7 | async-start | bytes 1376256 | tf_op jit(solution)/shard_map/reduce_scatter | solution.py:31
  315.1 151.8 %all-to-all-start.2 = ((bf16[16,7,2048]{2,1,0:T(8,128)(2,1)}), bf16[16,7,2048]{2,1,0:T(8,128)(2,1)S(1)}, u32[]{:S(2)}, u32[]{:S(2)}) async-start(bf16[16,7,2048]{2,1,0:T(8,128)(2,1)} %reshape.469), calls=%async_computation.4 | async-start | bytes 1048576 | tf_op jit(solution)/shard_map/all_to_all | solution.py:168
  325.2 3.4 copy-start.1
  334.2 3.4 copy-start.1
  343.3 3.4 copy-start.1
  352.3 3.4 copy-start.1
  361.4 3.4 copy-start.1
  370.4 3.4 copy-start.1
  379.5 3.4 copy-start.1
  388.5 3.4 copy-start.1
  397.6 3.4 copy-start.1
  406.6 3.4 copy-start.1
  415.7 3.4 copy-start.1
  424.7 3.4 copy-start.1
  433.8 3.4 copy-start.1
  442.8 3.4 copy-start.1
  451.9 3.4 copy-start.1
  460.9 3.4 copy-start.1
  466.2 4.0 copy-start.2
  466.2 4.4 copy-start.5
Sparse Core Ops, SparseCore 0:
  219.7 77.8 reduce-scatter.2
  300.1 13.0 reduce-scatter.4
Sparse Core Ops, SparseCore 1:
  223.8 48.9 all-gather.1
